TPU v7x, 512 devices: a whole 4x8x8 slice. The times are simulated.
512 devices in a mesh: kv: 128 (over z, y, core), tp: 4 (over x).
Axes of the slice: x: 4, y: 8, z: 8, core: 2. Of those that a mesh axis runs over, the one named last changes fastest.
Arguments:
- piece_tokens: bfloat16 [512, 2048], P('kv'), may hold values from -6 to 6
- decode_tokens: bfloat16 [128, 2048], P('kv'), may hold values from -6 to 6
- prompt_fill: int32 [1], replicated, may hold values from 16384 to 32256
- decode_fill: int32 [128], P('kv'), may hold values from 1 to 767, 49152 in all
- prompt_cache: bfloat16 [32768, 544], P('kv'), may hold values from -600 to 600
- decode_cache: bfloat16 [128, 768, 544], P('kv'), may hold values from -600 to 600
- input_gain: float32 [2048], replicated, may hold values from 0.1 to 1.9
- query_gain: float32 [768], replicated, may hold values from 0.1 to 1.9
- latent_gain: float32 [512], replicated, may hold values from 0.1 to 1.9
- query_down: bfloat16 [2048, 768], P(None, 'tp'), may hold values from -0.125 to 0.125
- latent_down: bfloat16 [2048, 512], P(None, 'tp'), may hold values from -0.125 to 0.125
- rope_down: bfloat16 [2048, 32], replicated, may hold values from -0.125 to 0.125
- query_up: bfloat16 [768, 1024], P(None, 'tp'), may hold values from -0.21875 to 0.21875
- qrope_up: bfloat16 [768, 512], P(None, 'tp'), may hold values from -0.21875 to 0.21875
- key_up: bfloat16 [16, 64, 512], P('tp'), may hold values from -0.25 to 0.25
- value_up: bfloat16 [16, 512, 64], P('tp'), may hold values from -4 to 4
- out_proj: bfloat16 [1024, 2048], P('tp'), may hold values from -4 to 4
Outputs:
- piece_out: bfloat16 [512, 2048], P('kv')
- decode_out: bfloat16 [128, 2048], P('kv')
- piece_rows: bfloat16 [512, 544], P('kv')
- decode_rows: bfloat16 [128, 544], P('kv')
Inputs may be any that keep to these rules, and one draw needn't show every extreme that they name: `prompt_fill`: the piece takes the 512 positions that follow the cache's filled positions. `decode_fill`: a decoding sequence's new token takes the position that follows its filled ones.
All inputs are finite; a program needn't handle non-finite values. No bound on the sum of `decode_fill` on one device may be relied on, other than what follows from the above.
Results may differ from a plain program's by a relative error of at most 0.035.
Values may be sent and summed in bfloat16 or wider, within the bound.
A program may use at most 64 MiB of HBM per device.

v0:
```python
import functools
import math

import jax
import jax.numpy as jnp
from jax import lax
from jax.experimental import pallas as pl
from jax.experimental.pallas import tpu as pltpu
from jax.sharding import PartitionSpec as P

NOPE = 64
ROPE = 32
NEG_FILL = -1e30
RMS_EPS = 1e-06
THETA = 10000.0
F32 = jnp.float32
BF16 = jnp.bfloat16
MESH = pl.DeviceIdType.MESH


def dot(a, b):
    return jnp.dot(a, b, preferred_element_type=F32)


def dot_t(a, b):
    return lax.dot_general(a, b, (((1,), (1,)), ((), ())), preferred_element_type=F32)


def each(low, high, body):
    if high - low <= 8:
        for i in range(low, high):
            body(i)
    else:
        lax.fori_loop(low, high, lambda i, carry: (body(i), carry)[1], 0)


def round_up(value, step):
    return -(-value // step) * step


def kernel(
    n,
    m,
    pt_h,
    dt_h,
    pf_h,
    df_h,
    pc_h,
    dc_h,
    ig_h,
    qg_h,
    lg_h,
    qd_h,
    ld_h,
    rd_h,
    qu_h,
    ru_h,
    ku_h,
    vu_h,
    op_h,
    po_ref,
    do_ref,
    pr_ref,
    dr_ref,
    tok,
    dtok,
    pfill,
    dfill,
    kbuf,
    dbuf,
    ig,
    qg,
    lg,
    qd,
    ld,
    rd,
    qu,
    ru,
    ku,
    vu,
    op,
    x,
    qall,
    lx,
    qx,
    stage,
    csend,
    crecv,
    dbuf_out,
    outs,
    in_sem,
    q_sem,
    l_sem,
    c_sem,
    d_sem,
    o_sem,
):
    me = lax.axis_index("kv")
    mt = lax.axis_index("tp")
    p = tok.shape[0]
    dd = dtok.shape[0]
    own = lx.shape[1]
    extra = x.shape[0]
    rows = qx.shape[1]
    cache = pc_h.shape[1]
    slots = dc_h.shape[2]
    heads = ku.shape[0]
    kl = ku.shape[2]
    key_width = kbuf.shape[0]
    part_q = qd.shape[0]
    part_l = ld.shape[1]
    ql = qu.shape[0]
    chunks = len(outs)
    chunk = outs[0].shape[2]

    pairs = [
        (pt_h, tok),
        (dt_h, dtok),
        (ig_h, ig),
        (qd_h, qd),
        (ld_h, ld),
        (rd_h, rd),
        (pf_h, pfill),
        (df_h, dfill),
        (qg_h, qg),
        (lg_h, lg),
        (qu_h, qu),
        (ru_h, ru),
        (ku_h, ku),
        (pc_h, kbuf),
        (vu_h, vu),
        (dc_h, dbuf),
        (op_h, op),
    ]
    loads = [pltpu.make_async_copy(s, d, in_sem.at[i]) for i, (s, d) in enumerate(pairs)]
    for load in loads:
        load.start()
    early, late, last = loads[:6], loads[6:-1], loads[-1]

    barrier = pltpu.get_barrier_semaphore()

    def greet(dk, dt):
        pl.semaphore_signal(
            barrier,
            inc=1,
            device_id=(lax.rem(me + dk, n), lax.rem(mt + dt, m)),
            device_id_type=MESH,
        )

    for dt in range(m):
        each(0 if dt else 1, n, lambda dk, dt=dt: greet(dk, dt))

    x[...] = jnp.zeros_like(x)
    for load in early:
        load.wait()
    x[0:p, :] = tok[...].astype(F32)
    x[p : p + dd, :] = dtok[...].astype(F32)
    xs = x[...]
    normed = (
        xs * lax.rsqrt(jnp.mean(xs * xs, axis=-1, keepdims=True) + RMS_EPS) * ig[...]
    ).astype(BF16)
    columns = dot_t(normed, qd[...])[0:own]
    qall[mt, 0] = columns[0:p].astype(BF16)
    lx[mt] = jnp.concatenate([dot(normed, ld[...])[0:own], columns], axis=1).astype(BF16)
    raw = dot_t(normed, rd[...])[0:own].astype(BF16).astype(F32)

    pl.semaphore_wait(barrier, n * m - 1)

    def query_copy(dk, dt):
        return pltpu.make_async_remote_copy(
            src_ref=qall.at[mt, 0],
            dst_ref=qall.at[mt, dk],
            send_sem=q_sem.at[0, dt, dk],
            recv_sem=q_sem.at[1, dt, dk],
            device_id=(lax.rem(me + dk, n), lax.rem(mt + dt, m)),
            device_id_type=MESH,
        )

    for dt in range(m):
        each(1, n, lambda dk, dt=dt: query_copy(dk, dt).start())
    l_copies = []
    for dt in range(1, m):
        copy = pltpu.make_async_remote_copy(
            src_ref=lx.at[mt],
            dst_ref=lx.at[mt],
            send_sem=l_sem.at[0, dt],
            recv_sem=l_sem.at[1, dt],
            device_id=(me, lax.rem(mt + dt, m)),
            device_id_type=MESH,
        )
        copy.start()
        l_copies.append(copy)

    for load in late:
        load.wait()
    fill = pfill[...]
    row = lax.broadcasted_iota(jnp.int32, (rows, 1), 0)
    slot = jnp.zeros((rows, 1), jnp.int32)
    for d in range(1, n):
        slot = jnp.where(row >= own + (d - 1) * p, d, slot)
    source = me - slot
    source = jnp.where(source < 0, source + n, source)
    inside = jnp.where(slot == 0, row, row - own - (slot - 1) * p)
    places = fill + source * p + inside
    for b in range(dd):
        places = jnp.where(row == p + b, dfill[b : b + 1, :], places)
    half = ROPE // 2
    turned_axis = heads * ROPE
    lane = lax.broadcasted_iota(jnp.int32, (1, turned_axis), 1)
    frequency = jnp.zeros((1, turned_axis), F32)
    for i in range(half):
        frequency = jnp.where(lane % half == i, THETA ** (-i / half), frequency)
    angles = places.astype(F32) * frequency
    cosine = jnp.cos(angles)
    sine = jnp.sin(angles)
    cos_own = cosine[0:own, 0:half]
    sin_own = sine[0:own, 0:half]
    first, second = raw[:, 0:half], raw[:, half:ROPE]
    new_rope = jnp.concatenate(
        [first * cos_own - second * sin_own, first * sin_own + second * cos_own], axis=1
    )
    gains = qg[...].reshape(1, ql)
    qx[...] = jnp.zeros_like(qx)

    for copy in l_copies:
        copy.wait_recv()
    latent = jnp.concatenate([lx[s, :, 0:part_l].astype(F32) for s in range(m)], axis=1)
    latent = (
        latent * lax.rsqrt(jnp.mean(latent * latent, axis=-1, keepdims=True) + RMS_EPS) * lg[...]
    )
    new_rows = jnp.concatenate([latent, new_rope], axis=1)
    pr_ref[...] = new_rows[0:p].astype(BF16)
    dr_ref[...] = new_rows[p : p + dd].astype(BF16)
    new_bf = jnp.concatenate([new_rows, jnp.zeros((extra - own, key_width), F32)], axis=0)
    new_bf = new_bf.astype(BF16)
    new_latent, new_key = new_bf[:, 0:kl], new_bf[:, kl:key_width]
    for s in range(m):
        qx[s, 0:own, :] = lx[s, :, part_l:].astype(F32)

    for dt in range(m):
        each(1, n, lambda dk, dt=dt: query_copy(dk, dt).wait_recv())
    for d in range(1, n):
        start = own + (d - 1) * p
        qx[:, start : start + p, :] = qall[:, d].astype(F32)
    parts = [qx[s] for s in range(m)]
    square = sum(jnp.sum(v * v, axis=-1, keepdims=True) for v in parts)
    scale = lax.rsqrt(square / ql + RMS_EPS)
    nope = jnp.zeros((rows, qu.shape[1]), F32)
    turn = jnp.zeros((rows, ru.shape[1]), F32)
    for s in range(m):
        lat = (parts[s] * scale * gains[:, s * part_q : (s + 1) * part_q]).astype(BF16)
        nope += dot(lat, qu[s * part_q : (s + 1) * part_q, :])
        turn += dot(lat, ru[s * part_q : (s + 1) * part_q, :])
    nope = nope.astype(BF16)
    turn = turn.astype(BF16).astype(F32)
    above = pltpu.roll(turn, turned_axis - half, 1)
    below = pltpu.roll(turn, half, 1)
    turned = turn * cosine + jnp.where(lane % ROPE < half, -above, below) * sine
    nd = qu.shape[1] // heads
    absorbed = [dot(nope[:, h * nd : (h + 1) * nd], ku[h]) for h in range(heads)]
    turned = [turned[:, h * ROPE : (h + 1) * ROPE] for h in range(heads)]

    score_scale = (NOPE + ROPE) ** (-0.5)
    aq = jnp.concatenate(absorbed, axis=0).astype(BF16)
    tq = jnp.concatenate(turned, axis=0).astype(BF16)
    scores = (
        jnp.concatenate(
            [
                dot(aq, kbuf[0:kl]) + dot(tq, kbuf[kl:key_width]),
                dot_t(aq, new_latent) + dot_t(tq, new_key),
            ],
            axis=1,
        )
        * score_scale
    )
    key = lax.broadcasted_iota(jnp.int32, (1, cache + extra), 1)
    query_place = jnp.concatenate([places] * heads, axis=0)
    fresh = key - cache
    never = jnp.int32(2**30)
    stored = jnp.where(me * cache + key < fill, me * cache + key, never)
    key_place = jnp.where(fresh < 0, stored, jnp.where(fresh < p, fill + me * p + fresh, never))
    allowed = key_place <= query_place
    scores = jnp.where(allowed, scores, NEG_FILL)
    peak = jnp.max(scores, axis=-1, keepdims=True)
    weights = jnp.where(allowed, jnp.exp(scores - peak), 0.0)
    total = jnp.sum(weights, axis=-1, keepdims=True)
    weights = weights.astype(BF16)
    mixed = dot_t(weights[:, 0:cache], kbuf[0:kl]) + dot(weights[:, cache:], new_latent)
    vd = vu.shape[1]
    peak_high = peak.astype(BF16).astype(F32)
    peak_mid = (peak - peak_high).astype(BF16).astype(F32)
    peak_low = peak - peak_high - peak_mid
    total_high = total.astype(BF16).astype(F32)
    total_low = total - total_high
    stat_lane = lax.broadcasted_iota(jnp.int32, (1, csend.shape[2] - vd), 1)
    stats = jnp.where(stat_lane == 0, peak_high, total_low)
    stats = jnp.where(stat_lane == 1, peak_mid, stats)
    stats = jnp.where(stat_lane == 2, peak_low, stats)
    stats = jnp.where(stat_lane == 3, total_high, stats)
    for h in range(heads):
        cut = slice(h * rows, (h + 1) * rows)
        message = jnp.concatenate([dot_t(mixed[cut].astype(BF16), vu[h]), stats[cut]], axis=1)
        stage[0, h * p : (h + 1) * p, :] = message[0:p]
        for d in range(1, n):
            start = own + (d - 1) * p
            stage[d, h * p : (h + 1) * p, :] = message[start : start + p]
    csend[...] = stage[...].astype(BF16)

    def value_copy(d):
        return pltpu.make_async_remote_copy(
            src_ref=csend.at[d],
            dst_ref=crecv.at[d],
            send_sem=c_sem.at[0, d],
            recv_sem=c_sem.at[1, d],
            device_id=(lax.rem(me + n - d, n), mt),
            device_id_type=MESH,
        )

    each(1, n, lambda d: value_copy(d).start())

    dvalues = []
    for b in range(dd):
        at = slice(p + b, p + b + 1)
        qa = jnp.concatenate([v[at] for v in absorbed], axis=0).astype(BF16)
        qt = jnp.concatenate([v[at] for v in turned], axis=0).astype(BF16)
        ds = (
            jnp.concatenate(
                [
                    dot(qa, dbuf[b, 0:kl]) + dot(qt, dbuf[b, kl:key_width]),
                    dot_t(qa, new_latent) + dot_t(qt, new_key),
                ],
                axis=1,
            )
            * score_scale
        )
        dk = lax.broadcasted_iota(jnp.int32, ds.shape, 1)
        ok = (dk < jnp.minimum(dfill[b : b + 1, :], slots)) | (dk == slots + p + b)
        ds = jnp.where(ok, ds, NEG_FILL)
        dpeak = jnp.max(ds, axis=-1, keepdims=True)
        dw = jnp.where(ok, jnp.exp(ds - dpeak), 0.0)
        dtotal = jnp.sum(dw, axis=-1, keepdims=True)
        dw = dw.astype(BF16)
        dmix = (dot_t(dw[:, 0:slots], dbuf[b, 0:kl]) + dot(dw[:, slots:], new_latent)).astype(BF16)
        dvals = [dot_t(dmix, vu[h])[h : h + 1] / dtotal[h : h + 1] for h in range(heads)]
        dvalues.append(jnp.concatenate(dvals, axis=1))
    last.wait()

    def row_copy(buf, sem, dt):
        return pltpu.make_async_remote_copy(
            src_ref=buf.at[mt],
            dst_ref=buf.at[mt],
            send_sem=sem.at[0, dt],
            recv_sem=sem.at[1, dt],
            device_id=(me, lax.rem(mt + dt, m)),
            device_id_type=MESH,
        )

    dbuf_out[mt] = dot(jnp.concatenate(dvalues, axis=0).astype(BF16), op[...]).astype(BF16)
    o_copies = [row_copy(dbuf_out, d_sem, dt) for dt in range(1, m)]
    for copy in o_copies:
        copy.start()

    each(1, n, lambda d: value_copy(d).wait_recv())
    blocks = [csend[0].astype(F32)] + [crecv[d].astype(F32) for d in range(1, n)]

    def peak_of(block):
        return block[:, vd : vd + 1] + block[:, vd + 1 : vd + 2] + block[:, vd + 2 : vd + 3]

    peaks = [peak_of(block) for block in blocks]
    top = functools.reduce(jnp.maximum, peaks)
    merged = jnp.zeros(blocks[0].shape, F32)
    for block, block_peak in zip(blocks, peaks):
        merged += block * jnp.exp(block_peak - top)
    value = merged[:, 0:vd] / (merged[:, vd + 3 : vd + 4] + merged[:, vd + 4 : vd + 5])
    values = jnp.concatenate([value[h * p : (h + 1) * p] for h in range(heads)], axis=1)
    values = values.astype(BF16)
    for c in range(chunks):
        obuf = outs[c]
        obuf[mt] = dot(values, op[:, c * chunk : (c + 1) * chunk]).astype(BF16)
        for dt in range(1, m):
            copy = row_copy(obuf, o_sem.at[c], dt)
            copy.start()
            o_copies.append(copy)
    for copy in o_copies:
        copy.wait_recv()
    do_ref[...] = sum(dbuf_out[s].astype(F32) for s in range(m)).astype(BF16)
    for c in range(chunks):
        out = sum(outs[c][s].astype(F32) for s in range(m))
        po_ref[:, c * chunk : (c + 1) * chunk] = out.astype(BF16)
    for dt in range(m):
        each(1, n, lambda dk, dt=dt: query_copy(dk, dt).wait_send())
    each(1, n, lambda d: value_copy(d).wait_send())
    for copy in l_copies + o_copies:
        copy.wait_send()


def put_out(*refs):
    count = len(refs) // 2
    sem = refs[-1]
    copies = [
        pltpu.make_async_copy(refs[i], refs[count + i], sem.at[i]) for i in range(count)
    ]
    for copy in copies:
        copy.start()
    for copy in copies:
        copy.wait()


def local(n, m, *args):
    (pt, dt, pfill, dfill, pc, dc, ig, qg, lg, qd, ld, rd, qu, ru, ku, vu, op) = args
    p, width = pt.shape
    dd = dt.shape[0]
    own = round_up(p + dd, 8)
    rows = round_up(own + (n - 1) * p, 8)
    extra = round_up(own, 16)
    heads, nd, kl = ku.shape
    chunks = 2
    any_spec = pl.BlockSpec(memory_space=pltpu.HBM)
    vmem = pl.BlockSpec(memory_space=pltpu.VMEM)
    ig, lg = ig[None], lg[None]
    pfill, dfill = pfill[None], dfill[:, None]
    pc, qd, rd = pc.T, qd.T, rd.T
    dc, vu = jnp.swapaxes(dc, 1, 2), jnp.swapaxes(vu, 1, 2)
    like = lambda a: pltpu.VMEM(a.shape, a.dtype)
    scratch = [
        *[like(a) for a in (pt, dt, pfill, dfill, pc, dc, ig, qg, lg)],
        *[like(a) for a in (qd, ld, rd, qu, ru, ku, vu, op)],
        pltpu.VMEM((extra, width), F32),
        pltpu.VMEM((m, n, p, qd.shape[0]), BF16),
        pltpu.VMEM((m, own, ld.shape[1] + qd.shape[0]), BF16),
        pltpu.VMEM((m, rows, qd.shape[0]), F32),
        pltpu.VMEM((n, heads * p, 128), F32),
        pltpu.VMEM((n, heads * p, 128), BF16),
        pltpu.VMEM((n, heads * p, 128), BF16),
        pltpu.VMEM((m, dd, width), BF16),
        [pltpu.VMEM((m, p, width // chunks), BF16)] * chunks,
        pltpu.SemaphoreType.DMA((17,)),
        pltpu.SemaphoreType.DMA((2, m, n)),
        pltpu.SemaphoreType.DMA((2, m)),
        pltpu.SemaphoreType.DMA((2, n)),
        pltpu.SemaphoreType.DMA((2, m)),
        pltpu.SemaphoreType.DMA((chunks, 2, m)),
    ]
    held = pl.pallas_call(
        functools.partial(kernel, n, m),
        out_shape=(
            pltpu.VMEM((p, width), BF16),
            pltpu.VMEM((dd, width), BF16),
            pltpu.VMEM((p, pc.shape[0]), BF16),
            pltpu.VMEM((dd, pc.shape[0]), BF16),
        ),
        in_specs=[any_spec] * 17,
        out_specs=(vmem,) * 4,
        scratch_shapes=scratch,
        compiler_params=pltpu.CompilerParams(
            collective_id=0, has_side_effects=True, vmem_limit_bytes=60 * 1024 * 1024
        ),
    )(pt, dt, pfill, dfill, pc, dc, ig, qg, lg, qd, ld, rd, qu, ru, ku, vu, op)
    return pl.pallas_call(
        put_out,
        out_shape=tuple(jax.ShapeDtypeStruct(a.shape, a.dtype) for a in held),
        in_specs=[vmem] * len(held),
        out_specs=(any_spec,) * len(held),
        scratch_shapes=[pltpu.SemaphoreType.DMA((len(held),))],
        compiler_params=pltpu.CompilerParams(vmem_limit_bytes=1024 * 1024),
    )(*held)


def solution(mesh):
    placed = (
        P("kv", None),
        P("kv", None),
        P(),
        P("kv"),
        P("kv", None),
        P("kv", None, None),
        P(),
        P(),
        P(),
        P(None, "tp"),
        P(None, "tp"),
        P(),
        P(None, "tp"),
        P(None, "tp"),
        P("tp", None, None),
        P("tp", None, None),
        P("tp", None),
    )
    return jax.shard_map(
        functools.partial(local, mesh.shape["kv"], mesh.shape["tp"]),
        mesh=mesh,
        in_specs=placed,
        out_specs=(P("kv", None), P("kv", None), P("kv", None), P("kv", None)),
        check_vma=False,
    )
```

profile of v0, /device:TPU:1, one launch (start us, length us, event | category | flops | bytes accessed | tf_op | source)
XLA Modules:
  0.0 101.8 jit_solution(4383122103174760032)
XLA Ops:
  1.9 99.3 %shard_map.192 = (bf16[4,2048]{1,0:T(4,128)(2,1)S(1)}, bf16[1,2048]{1,0:T(2,128)(2,1)S(1)}, bf16[4,544]{1,0:T(4,128)(2,1)S(1)}, bf16[1,544]{1,0:T(2,128)(2,1)S(1)}) custom-call(bf16[4,2048]{1,0:T(4,128)(2,1)} %pt_h.1, bf16[1,2048]{1,0:T(2,128)(2,1)} %dt_h.1, s32[1,1]{1,0:T(1,128)} %bitcast.9.pf_h, s32[1,1]{1,0:T(1,128)} %bitcast.10.df_h, ...), custom_call_target="tpu_custom_call" | custom-call | tf_op jit(solution)/shard_map/pallas_call | solution.py:444
  101.2 0.6 shard_map.193
where the time goes:
time: 102 us
  Pallas kernels  99.9 us (98%)
  between operations  1.94 us (2%)
    pallas_call x1, Pallas kernels, local(): pl.pallas_call(functools.partial(kernel, n, m), out_shape=(pltpu.VMEM((p,...  99.3 us

commit v1 on v0

v1 whole, which is shorter than its diff:
```python
import functools
import math

import jax
import jax.numpy as jnp
from jax import lax
from jax.experimental import pallas as pl
from jax.experimental.pallas import tpu as pltpu
from jax.sharding import PartitionSpec as P

NOPE = 64
ROPE = 32
CORES = 2
NEG_FILL = -1e30
RMS_EPS = 1e-06
THETA = 10000.0
SCALE2 = (NOPE + ROPE) ** (-0.5) * math.log2(math.e)
F32 = jnp.float32
BF16 = jnp.bfloat16
MESH = pl.DeviceIdType.MESH


def dot(a, b):
    return jnp.dot(a, b, preferred_element_type=F32)


def dot_t(a, b):
    return lax.dot_general(a, b, (((1,), (1,)), ((), ())), preferred_element_type=F32)


def each(low, high, body):
    if high - low <= 4:
        for i in range(low, high):
            body(i)
    else:
        lax.fori_loop(low, high, lambda i, carry: (body(i), carry)[1], 0)


def far_first(j, count):
    return count // 2 + ((j + 1) // 2) * (1 - 2 * (j % 2))


def kernel(
    n,
    m,
    pt_h,
    dt_h,
    pf_h,
    df_h,
    pc_h,
    dc_h,
    ig_h,
    qg_h,
    lg_h,
    qd_h,
    ld_h,
    rd_h,
    qu_h,
    ru_h,
    ku_h,
    vu_h,
    op_h,
    po_ref,
    do_ref,
    pr_ref,
    dr_ref,
    tok,
    dtok,
    pfill,
    dfill,
    kbuf,
    dbuf,
    ig,
    qg,
    lg,
    qd,
    ld,
    rd,
    qu,
    ru,
    ku,
    vu,
    op,
    x,
    lx,
    qbuf,
    nbuf,
    krt,
    vt,
    csend,
    crecv,
    dbuf_out,
    outs,
    in_sem,
    q_sem,
    l_sem,
    c_sem,
    p_sem,
    d_sem,
    o_sem,
):
    me = lax.axis_index("kv")
    mt = lax.axis_index("tp")
    chips = n // CORES
    ny = math.isqrt(chips)
    nz = chips // ny
    chip = me // CORES
    core = me % CORES
    peer = me + 1 - 2 * core
    z, y = chip // ny, chip % ny
    p = tok.shape[0]
    dd = dtok.shape[0]
    own = lx.shape[1]
    extra = x.shape[0]
    cache = pc_h.shape[1]
    slots = dc_h.shape[2]
    heads = ku.shape[0]
    kl = ku.shape[2]
    key_width = pc_h.shape[0]
    part_q = qd.shape[0]
    part_l = ld.shape[1]
    ql = qu.shape[0]
    block = heads * p
    chunks = len(outs)
    chunk = outs[0].shape[2]
    half_lanes = 64

    pairs = [
        (pt_h, tok),
        (dt_h, dtok),
        (ig_h, ig),
        (qd_h, qd),
        (ld_h, ld),
        (rd_h, rd),
        (pc_h, kbuf.at[0]),
        (ku_h, ku),
        (vu_h, vu),
        (pf_h, pfill),
        (df_h, dfill),
        (qg_h, qg),
        (lg_h, lg),
        (qu_h, qu),
        (ru_h, ru),
        (dc_h, dbuf),
        (op_h, op),
    ]
    loads = [pltpu.make_async_copy(s, d, in_sem.at[i]) for i, (s, d) in enumerate(pairs)]
    for load in loads:
        load.start()
    early, middle, late, last = loads[:6], loads[6:11], loads[11:15], loads[15:]

    barrier = pltpu.get_barrier_semaphore()

    def other(i):
        dz, dy = far_first(i // ny, nz), far_first(i % ny, ny)
        to = ((z + dz) % nz) * ny + (y + dy) % ny
        source = ((z + nz - dz) % nz) * ny + (y + ny - dy) % ny
        return to, source

    def greet(kv, tp):
        pl.semaphore_signal(barrier, inc=1, device_id=(kv, tp), device_id_type=MESH)

    each(0, chips - 1, lambda i: greet(other(i)[0] * CORES + core, mt))
    greet(peer, mt)
    for dt in range(1, m):
        greet(me, lax.rem(mt + dt, m))

    x[...] = jnp.zeros_like(x)
    for load in early:
        load.wait()
    x[0:p, :] = tok[...].astype(F32)
    x[p : p + dd, :] = dtok[...].astype(F32)
    xs = x[...]
    normed = (
        xs * lax.rsqrt(jnp.mean(xs * xs, axis=-1, keepdims=True) + RMS_EPS) * ig[...]
    ).astype(BF16)
    columns = dot_t(normed, qd[...])[0:own]
    lx[mt] = jnp.concatenate([dot(normed, ld[...])[0:own], columns], axis=1).astype(BF16)
    raw = dot_t(normed, rd[...])[0:own].astype(BF16).astype(F32)

    for load in middle:
        load.wait()
    fill = pfill[...]
    row = lax.broadcasted_iota(jnp.int32, (own, 1), 0)
    places = fill + me * p + row
    for b in range(dd):
        places = jnp.where(row == p + b, dfill[b : b + 1, :], places)
    half = ROPE // 2
    lane = lax.broadcasted_iota(jnp.int32, (1, heads * ROPE), 1)
    frequency = jnp.zeros((1, heads * ROPE), F32)
    for i in range(half):
        frequency = jnp.where(lane % half == i, THETA ** (-i / half), frequency)
    angles = places.astype(F32) * frequency
    cosine = jnp.cos(angles)
    sine = jnp.sin(angles)
    cos_own = cosine[:, 0:half]
    sin_own = sine[:, 0:half]
    first, second = raw[:, 0:half], raw[:, half:ROPE]
    new_rope = jnp.concatenate(
        [first * cos_own - second * sin_own, first * sin_own + second * cos_own], axis=1
    )

    key_up = ku[...].reshape(heads * NOPE, kl)
    value_up = vu[...].reshape(vu.shape[0] * vu.shape[1], kl)

    def expand(slot, owner):
        at = slice(slot * cache, (slot + 1) * cache)
        latent_t = kbuf[slot, 0:kl]
        rope_t = kbuf[slot, kl:key_width]
        krt[0 : heads * NOPE, at] = dot(key_up, latent_t).astype(BF16)
        vt[:, at] = dot(value_up, latent_t).astype(BF16)
        sub = lax.broadcasted_iota(jnp.int32, (ROPE, cache), 0)
        place = owner * cache + lax.broadcasted_iota(jnp.int32, (ROPE, cache), 1)
        bias = jnp.where((sub == 0) & (place >= fill), NEG_FILL, 0.0).astype(BF16)
        krt[heads * NOPE :, at] = jnp.concatenate([rope_t, bias, rope_t, bias], axis=0)

    expand(0, me)

    pl.semaphore_wait(barrier, chips - 1 + 1 + m - 1)

    l_copies = []
    for dt in range(1, m):
        copy = pltpu.make_async_remote_copy(
            src_ref=lx.at[mt],
            dst_ref=lx.at[mt],
            send_sem=l_sem.at[0, dt],
            recv_sem=l_sem.at[1, dt],
            device_id=(me, lax.rem(mt + dt, m)),
            device_id_type=MESH,
        )
        copy.start()
        l_copies.append(copy)

    def peer_copy(src, dst, index):
        return pltpu.make_async_remote_copy(
            src_ref=src,
            dst_ref=dst,
            send_sem=p_sem.at[0, index],
            recv_sem=p_sem.at[1, index],
            device_id=(peer, mt),
            device_id_type=MESH,
        )

    cache_copy = peer_copy(kbuf.at[0], kbuf.at[1], 0)
    cache_copy.start()
    for load in late:
        load.wait()
    gains = qg[...].reshape(1, ql)

    for copy in l_copies:
        copy.wait_recv()
    parts = [lx[s, :, part_l:].astype(F32) for s in range(m)]
    square = sum(jnp.sum(v * v, axis=-1, keepdims=True) for v in parts)
    scale = lax.rsqrt(square / ql + RMS_EPS)
    nope = jnp.zeros((own, qu.shape[1]), F32)
    turn = jnp.zeros((own, ru.shape[1]), F32)
    for s in range(m):
        lat = (parts[s] * scale * gains[:, s * part_q : (s + 1) * part_q]).astype(BF16)
        nope += dot(lat, qu[s * part_q : (s + 1) * part_q, :])
        turn += dot(lat, ru[s * part_q : (s + 1) * part_q, :])
    nope = nope.astype(BF16).astype(F32)
    turn = turn.astype(BF16).astype(F32)
    turned_axis = heads * ROPE
    above = pltpu.roll(turn, turned_axis - half, 1)
    below = pltpu.roll(turn, half, 1)
    turned = turn * cosine + jnp.where(lane % ROPE < half, -above, below) * sine
    blocks = []
    for h in range(heads):
        base = half_lanes * (1 - h % 2)
        shift = (base - h * ROPE) % 128
        moved = pltpu.roll(turned, shift, 1) if shift else turned
        tile = nope[:, (h // 2) * 128 : (h // 2 + 1) * 128]
        rest = jnp.where(lane < base + ROPE, moved, jnp.where(lane == base + ROPE, 1.0, 0.0))
        blocks.append(jnp.where((lane >= base) & (lane < base + half_lanes), rest, tile))
    message = jnp.concatenate([v[0:p] for v in blocks], axis=0).astype(BF16)
    own_rows = pl.ds(pl.multiple_of(chip * block, block), block)
    qbuf[own_rows, :] = message

    def rows_of(ref, index):
        return ref.at[pl.ds(pl.multiple_of(index * block, block), block)]

    def query_copy(i):
        to, source = other(i)
        return pltpu.make_async_remote_copy(
            src_ref=rows_of(qbuf, chip),
            dst_ref=rows_of(qbuf, chip),
            send_sem=q_sem.at[0, i],
            recv_sem=q_sem.at[1, i],
            device_id=(to * CORES + core, mt),
            device_id_type=MESH,
        )

    def query_arrival(i):
        to, source = other(i)
        return pltpu.make_async_remote_copy(
            src_ref=rows_of(qbuf, source),
            dst_ref=rows_of(qbuf, source),
            send_sem=q_sem.at[0, i],
            recv_sem=q_sem.at[1, i],
            device_id=(to * CORES + core, mt),
            device_id_type=MESH,
        )

    each(0, chips - 1, lambda i: query_copy(i).start())

    latent = jnp.concatenate([lx[s, :, 0:part_l].astype(F32) for s in range(m)], axis=1)
    latent = (
        latent * lax.rsqrt(jnp.mean(latent * latent, axis=-1, keepdims=True) + RMS_EPS) * lg[...]
    )
    new_rows = jnp.concatenate([latent, new_rope], axis=1)
    pr_ref[...] = new_rows[0:p].astype(BF16)
    dr_ref[...] = new_rows[p : p + dd].astype(BF16)
    new_bf = jnp.concatenate([new_rows, jnp.zeros((extra - own, key_width), F32)], axis=0)
    new_bf = new_bf.astype(BF16)
    nbuf[0] = new_bf
    rows_copy = peer_copy(nbuf.at[0], nbuf.at[1], 1)
    rows_copy.start()

    cache_copy.wait_recv()
    expand(1, peer)

    for load in last:
        load.wait()
    new_latent, new_key = new_bf[:, 0:kl], new_bf[:, kl:key_width]
    head_row = lax.broadcasted_iota(jnp.int32, (heads, heads * NOPE), 0)
    head_lane = lax.broadcasted_iota(jnp.int32, (heads, heads * NOPE), 1) // NOPE
    dvalues = []
    for b in range(dd):
        at = slice(p + b, p + b + 1)
        nope_rows = jnp.concatenate([nope[at]] * heads, axis=0)
        nope_rows = jnp.where(head_row == head_lane, nope_rows, 0.0).astype(BF16)
        qa = dot(nope_rows, key_up).astype(BF16)
        qt = jnp.concatenate(
            [turned[at, h * ROPE : (h + 1) * ROPE] for h in range(heads)], axis=0
        ).astype(BF16)
        ds = dot(qa, dbuf[b, 0:kl]) + dot(qt, dbuf[b, kl:key_width])
        df = dot_t(qa, new_latent) + dot_t(qt, new_key)
        dk = lax.broadcasted_iota(jnp.int32, ds.shape, 1)
        ds = jnp.where(dk < dfill[b : b + 1, :], ds, NEG_FILL)
        fk = lax.broadcasted_iota(jnp.int32, df.shape, 1)
        df = jnp.where(fk == p + b, df, NEG_FILL)
        dpeak = jnp.maximum(
            jnp.max(ds, axis=-1, keepdims=True), jnp.max(df, axis=-1, keepdims=True)
        )
        dw = jnp.exp2((ds - dpeak) * SCALE2)
        fw = jnp.exp2((df - dpeak) * SCALE2)
        dtotal = jnp.sum(dw, axis=-1, keepdims=True) + jnp.sum(fw, axis=-1, keepdims=True)
        dmix = dot_t(dw.astype(BF16), dbuf[b, 0:kl]) + dot(fw.astype(BF16), new_latent)
        dval = dot_t(dmix.astype(BF16), value_up) / dtotal
        dvalues.append(
            jnp.sum(jnp.where(head_row == head_lane, dval, 0.0), axis=0, keepdims=True)
        )

    def row_copy(buf, sem, dt):
        return pltpu.make_async_remote_copy(
            src_ref=buf.at[mt],
            dst_ref=buf.at[mt],
            send_sem=sem.at[0, dt],
            recv_sem=sem.at[1, dt],
            device_id=(me, lax.rem(mt + dt, m)),
            device_id_type=MESH,
        )

    dbuf_out[mt] = dot(jnp.concatenate(dvalues, axis=0).astype(BF16), op[...]).astype(BF16)
    o_copies = [row_copy(dbuf_out, d_sem, dt) for dt in range(1, m)]
    for copy in o_copies:
        copy.start()

    rows_copy.wait_recv()
    fresh = nbuf[...].reshape(2 * extra, key_width)
    fresh_rope = fresh[:, kl:key_width]
    gap = jnp.zeros((2 * extra, half_lanes - ROPE), BF16)
    fresh_key = jnp.concatenate(
        [dot_t(fresh[:, 0:kl], key_up).astype(BF16), fresh_rope, gap, fresh_rope, gap], axis=1
    )
    fresh_value = dot_t(fresh[:, 0:kl], value_up).astype(BF16)

    tile_rows = min(256, chips * block)
    lane_t = lax.broadcasted_iota(jnp.int32, (tile_rows, 128), 1)
    row_t = lax.broadcasted_iota(jnp.int32, (tile_rows, 128), 0)
    head_t = (row_t % block) // p
    low_t = lane_t < half_lanes
    even_t = head_t % 2 == 0
    is_nope = low_t == even_t
    pick = lambda mask: jnp.where(mask, 1.0, 0.0).astype(BF16)
    mask0 = pick(is_nope & (head_t < 2))
    mask1 = pick(is_nope & (head_t >= 2))
    mask_r = pick(jnp.logical_not(is_nope))
    frow = lax.broadcasted_iota(jnp.int32, (tile_rows, 2 * extra), 0)
    fcol = lax.broadcasted_iota(jnp.int32, (tile_rows, 2 * extra), 1)
    fplace = jnp.where(fcol < extra, me * p + fcol, peer * p + fcol - extra)
    freal = (fcol % extra) < p

    each(0, chips - 1, lambda i: query_arrival(i).wait_recv())

    for r0 in range(0, chips * block, tile_rows):
        rows = slice(r0, r0 + tile_rows)
        q = qbuf[rows, :]
        q = jnp.concatenate([q * mask0, q * mask1, q * mask_r], axis=1)
        s = dot(q, krt[...])
        sf = dot_t(q, fresh_key)
        qplace = ((r0 + frow) // block * CORES + core) * p + frow % p
        sf = jnp.where(freal & (fplace <= qplace), sf, NEG_FILL)
        peak = jnp.maximum(jnp.max(s, axis=-1, keepdims=True), jnp.max(sf, axis=-1, keepdims=True))
        w = jnp.exp2((s - peak) * SCALE2)
        wf = jnp.exp2((sf - peak) * SCALE2)
        total = jnp.sum(w, axis=-1, keepdims=True) + jnp.sum(wf, axis=-1, keepdims=True)
        o = dot_t(w.astype(BF16), vt[...]) + dot(wf.astype(BF16), fresh_value)
        o = jnp.where(head_t < 2, o[:, 0:128], o[:, 128:256])
        o = jnp.where(even_t, o, pltpu.roll(o, half_lanes, 1))
        level = peak * SCALE2 + jnp.log2(total)
        high = level.astype(BF16).astype(F32)
        mid = (level - high).astype(BF16).astype(F32)
        stats = jnp.where(lane_t == half_lanes, high, level - high - mid)
        stats = jnp.where(lane_t == half_lanes + 1, mid, stats)
        csend[rows, :] = jnp.where(low_t, o * (1.0 / total), stats).astype(BF16)

    def value_copy(i):
        to, source = other(i)
        return pltpu.make_async_remote_copy(
            src_ref=rows_of(csend, to),
            dst_ref=rows_of(crecv, chip),
            send_sem=c_sem.at[0, i],
            recv_sem=c_sem.at[1, i],
            device_id=(to * CORES + core, mt),
            device_id_type=MESH,
        )

    def value_arrival(i):
        to, source = other(i)
        return pltpu.make_async_remote_copy(
            src_ref=rows_of(csend, to),
            dst_ref=rows_of(crecv, source),
            send_sem=c_sem.at[0, i],
            recv_sem=c_sem.at[1, i],
            device_id=(to * CORES + core, mt),
            device_id_type=MESH,
        )

    each(0, chips - 1, lambda i: value_copy(i).start())
    crecv[own_rows, :] = csend[own_rows, :]

    for copy in o_copies:
        copy.wait_recv()
    do_ref[...] = sum(dbuf_out[s].astype(F32) for s in range(m)).astype(BF16)
    stat_row = lax.broadcasted_iota(jnp.int32, (128, 128), 0)
    summing = pick((stat_row >= half_lanes) & (stat_row < half_lanes + 3))

    each(0, chips - 1, lambda i: value_arrival(i).wait_recv())
    arrived = crecv[...]
    levels = dot(arrived, summing).reshape(chips, block, 128)
    arrived = arrived.astype(F32).reshape(chips, block, 128)
    top = jnp.max(levels, axis=0, keepdims=True)
    share = jnp.exp2(levels - top)
    value = jnp.sum(arrived * share, axis=0) / jnp.sum(share, axis=0)
    low = lax.broadcasted_iota(jnp.int32, (p, 128), 1) < half_lanes
    values = []
    for h in range(0, heads, 2):
        right = pltpu.roll(value[(h + 1) * p : (h + 2) * p], half_lanes, 1)
        values.append(jnp.where(low, value[h * p : (h + 1) * p], right))
    values = jnp.concatenate(values, axis=1).astype(BF16)
    p_copies = []
    for c in range(chunks):
        obuf = outs[c]
        obuf[mt] = dot(values, op[:, c * chunk : (c + 1) * chunk]).astype(BF16)
        for dt in range(1, m):
            copy = row_copy(obuf, o_sem.at[c], dt)
            copy.start()
            p_copies.append(copy)
    for c in range(chunks):
        for copy in p_copies[c * (m - 1) : (c + 1) * (m - 1)]:
            copy.wait_recv()
        out = sum(outs[c][s].astype(F32) for s in range(m))
        po_ref[:, c * chunk : (c + 1) * chunk] = out.astype(BF16)
    each(0, chips - 1, lambda i: query_copy(i).wait_send())
    each(0, chips - 1, lambda i: value_copy(i).wait_send())
    for copy in l_copies + [cache_copy, rows_copy] + o_copies + p_copies:
        copy.wait_send()


def put_out(*refs):
    count = len(refs) // 2
    sem = refs[-1]
    copies = [
        pltpu.make_async_copy(refs[i], refs[count + i], sem.at[i]) for i in range(count)
    ]
    for copy in copies:
        copy.start()
    for copy in copies:
        copy.wait()


def local(n, m, *args):
    (pt, dt, pfill, dfill, pc, dc, ig, qg, lg, qd, ld, rd, qu, ru, ku, vu, op) = args
    p, width = pt.shape
    dd = dt.shape[0]
    own = -(-(p + dd) // 8) * 8
    extra = 16
    heads, nd, kl = ku.shape
    block = heads * p
    chips = n // CORES
    chunks = 2
    any_spec = pl.BlockSpec(memory_space=pltpu.HBM)
    vmem = pl.BlockSpec(memory_space=pltpu.VMEM)
    ig, lg = ig[None], lg[None]
    pfill, dfill = pfill[None], dfill[:, None]
    pc, qd, rd = pc.T, qd.T, rd.T
    dc, vu = jnp.swapaxes(dc, 1, 2), jnp.swapaxes(vu, 1, 2)
    cache = pc.shape[1]
    like = lambda a: pltpu.VMEM(a.shape, a.dtype)
    scratch = [
        *[like(a) for a in (pt, dt, pfill, dfill)],
        pltpu.VMEM((2, *pc.shape), BF16),
        *[like(a) for a in (dc, ig, qg, lg)],
        *[like(a) for a in (qd, ld, rd, qu, ru, ku, vu, op)],
        pltpu.VMEM((extra, width), F32),
        pltpu.VMEM((m, own, ld.shape[1] + qd.shape[0]), BF16),
        pltpu.VMEM((chips * block, 128), BF16),
        pltpu.VMEM((2, extra, pc.shape[0]), BF16),
        pltpu.VMEM((heads * nd + 128, 2 * cache), BF16),
        pltpu.VMEM((heads * nd, 2 * cache), BF16),
        pltpu.VMEM((chips * block, 128), BF16),
        pltpu.VMEM((chips * block, 128), BF16),
        pltpu.VMEM((m, dd, width), BF16),
        [pltpu.VMEM((m, p, width // chunks), BF16)] * chunks,
        pltpu.SemaphoreType.DMA((17,)),
        pltpu.SemaphoreType.DMA((2, chips)),
        pltpu.SemaphoreType.DMA((2, m)),
        pltpu.SemaphoreType.DMA((2, chips)),
        pltpu.SemaphoreType.DMA((2, 2)),
        pltpu.SemaphoreType.DMA((2, m)),
        pltpu.SemaphoreType.DMA((chunks, 2, m)),
    ]
    held = pl.pallas_call(
        functools.partial(kernel, n, m),
        out_shape=(
            pltpu.VMEM((p, width), BF16),
            pltpu.VMEM((dd, width), BF16),
            pltpu.VMEM((p, pc.shape[0]), BF16),
            pltpu.VMEM((dd, pc.shape[0]), BF16),
        ),
        in_specs=[any_spec] * 17,
        out_specs=(vmem,) * 4,
        scratch_shapes=scratch,
        compiler_params=pltpu.CompilerParams(
            collective_id=0, has_side_effects=True, vmem_limit_bytes=60 * 1024 * 1024
        ),
    )(pt, dt, pfill, dfill, pc, dc, ig, qg, lg, qd, ld, rd, qu, ru, ku, vu, op)
    return pl.pallas_call(
        put_out,
        out_shape=tuple(jax.ShapeDtypeStruct(a.shape, a.dtype) for a in held),
        in_specs=[vmem] * len(held),
        out_specs=(any_spec,) * len(held),
        scratch_shapes=[pltpu.SemaphoreType.DMA((len(held),))],
        compiler_params=pltpu.CompilerParams(vmem_limit_bytes=1024 * 1024),
    )(*held)


def solution(mesh):
    placed = (
        P("kv", None),
        P("kv", None),
        P(),
        P("kv"),
        P("kv", None),
        P("kv", None, None),
        P(),
        P(),
        P(),
        P(None, "tp"),
        P(None, "tp"),
        P(),
        P(None, "tp"),
        P(None, "tp"),
        P("tp", None, None),
        P("tp", None, None),
        P("tp", None),
    )
    return jax.shard_map(
        functools.partial(local, mesh.shape["kv"], mesh.shape["tp"]),
        mesh=mesh,
        in_specs=placed,
        out_specs=(P("kv", None), P("kv", None), P("kv", None), P("kv", None)),
        check_vma=False,
    )
```

time: 102 us -> 50.3 us (0.49)
  the two profiles are of different devices: /device:TPU:1 before, /device:TPU:8 now
where the time goes in v1:
time: 50.3 us; the launch traced here: 50.1 us
  Pallas kernels  48.2 us (96%)
  between operations  1.94 us (4%)
    pallas_call x1, Pallas kernels, local(): pl.pallas_call(functools.partial(kernel, n, m), out_shape=(pltpu.VMEM((p,...  47.5 us

profile of v1, /device:TPU:8, one launch (start us, length us, event | category | flops | bytes accessed | tf_op | source)
XLA Modules:
  0.0 50.1 jit_solution(3737730378928685128)
XLA Ops:
  1.9 47.5 %shard_map.192 = (bf16[4,2048]{1,0:T(4,128)(2,1)S(1)}, bf16[1,2048]{1,0:T(2,128)(2,1)S(1)}, bf16[4,544]{1,0:T(4,128)(2,1)S(1)}, bf16[1,544]{1,0:T(2,128)(2,1)S(1)}) custom-call(bf16[4,2048]{1,0:T(4,128)(2,1)} %pt_h.1, bf16[1,2048]{1,0:T(2,128)(2,1)} %dt_h.1, s32[1,1]{1,0:T(1,128)} %bitcast.9.pf_h, s32[1,1]{1,0:T(1,128)} %bitcast.10.df_h, ...), custom_call_target="tpu_custom_call" | custom-call | tf_op jit(solution)/shard_map/pallas_call | solution.py:534
  49.5 0.6 %shard_map.193 = (bf16[4,2048]{1,0:T(4,128)(2,1)}, bf16[1,2048]{1,0:T(2,128)(2,1)}, bf16[4,544]{1,0:T(4,128)(2,1)}, bf16[1,544]{1,0:T(2,128)(2,1)}) custom-call(bf16[4,2048]{1,0:T(4,128)(2,1)S(1)} %get-tuple-element.8.refs_0_, bf16[1,2048]{1,0:T(2,128)(2,1)S(1)} %get-tuple-element.9.refs_1_, bf16[4,544]{1,0:T(4,128)(2,1)S(1)} %get-tuple-element.10.refs_2_, ...), custom_call_target="tpu_custom_call" | custom-call | tf_op jit(solution)/shard_map/pallas_call | solution.py:549

commit v2 on v1

--- a/solution.py
+++ b/solution.py
@@ -91,6 +91,7 @@
     crecv,
     dbuf_out,
     outs,
+    line_sem,
     in_sem,
     q_sem,
     l_sem,
@@ -160,7 +161,11 @@
     def greet(kv, tp):
         pl.semaphore_signal(barrier, inc=1, device_id=(kv, tp), device_id_type=MESH)
 
-    each(0, chips - 1, lambda i: greet(other(i)[0] * CORES + core, mt))
+    def along_z(dz):
+        return (((z + dz) % nz) * ny + y) * CORES + core
+
+    each(1, nz, lambda dz: greet(along_z(dz), mt))
+    each(1, ny, lambda dy: greet((z * ny + (y + dy) % ny) * CORES + core, mt))
     greet(peer, mt)
     for dt in range(1, m):
         greet(me, lax.rem(mt + dt, m))
@@ -180,11 +185,11 @@
 
     for load in middle:
         load.wait()
-    fill = pfill[...]
+    fill = pfill[0]
     row = lax.broadcasted_iota(jnp.int32, (own, 1), 0)
     places = fill + me * p + row
     for b in range(dd):
-        places = jnp.where(row == p + b, dfill[b : b + 1, :], places)
+        places = jnp.where(row == p + b, dfill[b], places)
     half = ROPE // 2
     lane = lax.broadcasted_iota(jnp.int32, (1, heads * ROPE), 1)
     frequency = jnp.zeros((1, heads * ROPE), F32)
@@ -216,7 +221,12 @@
 
     expand(0, me)
 
-    pl.semaphore_wait(barrier, chips - 1 + 1 + m - 1)
+    pl.semaphore_wait(barrier, nz - 1 + ny - 1 + 1 + m - 1)
+
+    def vouch(dz):
+        pl.semaphore_signal(line_sem, inc=1, device_id=(along_z(dz), mt), device_id_type=MESH)
+
+    each(1, nz, vouch)
 
     l_copies = []
     for dt in range(1, m):
@@ -301,6 +311,7 @@
             device_id_type=MESH,
         )
 
+    pl.semaphore_wait(line_sem, nz - 1)
     each(0, chips - 1, lambda i: query_copy(i).start())
 
     latent = jnp.concatenate([lx[s, :, 0:part_l].astype(F32) for s in range(m)], axis=1)
@@ -336,7 +347,7 @@
         ds = dot(qa, dbuf[b, 0:kl]) + dot(qt, dbuf[b, kl:key_width])
         df = dot_t(qa, new_latent) + dot_t(qt, new_key)
         dk = lax.broadcasted_iota(jnp.int32, ds.shape, 1)
-        ds = jnp.where(dk < dfill[b : b + 1, :], ds, NEG_FILL)
+        ds = jnp.where(dk < dfill[b], ds, NEG_FILL)
         fk = lax.broadcasted_iota(jnp.int32, df.shape, 1)
         df = jnp.where(fk == p + b, df, NEG_FILL)
         dpeak = jnp.maximum(
@@ -503,13 +514,13 @@
     any_spec = pl.BlockSpec(memory_space=pltpu.HBM)
     vmem = pl.BlockSpec(memory_space=pltpu.VMEM)
     ig, lg = ig[None], lg[None]
-    pfill, dfill = pfill[None], dfill[:, None]
     pc, qd, rd = pc.T, qd.T, rd.T
     dc, vu = jnp.swapaxes(dc, 1, 2), jnp.swapaxes(vu, 1, 2)
     cache = pc.shape[1]
     like = lambda a: pltpu.VMEM(a.shape, a.dtype)
     scratch = [
-        *[like(a) for a in (pt, dt, pfill, dfill)],
+        *[like(a) for a in (pt, dt)],
+        *[pltpu.SMEM(a.shape, a.dtype) for a in (pfill, dfill)],
         pltpu.VMEM((2, *pc.shape), BF16),
         *[like(a) for a in (dc, ig, qg, lg)],
         *[like(a) for a in (qd, ld, rd, qu, ru, ku, vu, op)],
@@ -523,6 +534,7 @@
         pltpu.VMEM((chips * block, 128), BF16),
         pltpu.VMEM((m, dd, width), BF16),
         [pltpu.VMEM((m, p, width // chunks), BF16)] * chunks,
+        pltpu.SemaphoreType.REGULAR,
         pltpu.SemaphoreType.DMA((17,)),
         pltpu.SemaphoreType.DMA((2, chips)),
         pltpu.SemaphoreType.DMA((2, m)),

time: 50.3 us -> 47.7 us (0.948)
  Pallas kernels: 48.2 us -> 45.6 us
    pallas_call x1, Pallas kernels: 47.5 us -> 45 us  [local(): pl.pallas_call(functools.partial(kernel, n, m), out_shape=(pltpu.VMEM((p,...]
where the time goes in v2:
time: 47.7 us; the launch traced here: 47.5 us
  Pallas kernels  45.6 us (96%)
  between operations  1.94 us (4%)
    pallas_call x1, Pallas kernels, local(): pl.pallas_call(functools.partial(kernel, n, m), out_shape=(pltpu.VMEM((p,...  45 us

profile of v2, /device:TPU:8, one launch (start us, length us, event | category | flops | bytes accessed | tf_op | source)
XLA Modules:
  0.0 47.5 jit_solution(12878062482089029640)
XLA Ops:
  1.9 45.0 %shard_map.192 = (bf16[4,2048]{1,0:T(4,128)(2,1)S(1)}, bf16[1,2048]{1,0:T(2,128)(2,1)S(1)}, bf16[4,544]{1,0:T(4,128)(2,1)S(1)}, bf16[1,544]{1,0:T(2,128)(2,1)S(1)}) custom-call(bf16[4,2048]{1,0:T(4,128)(2,1)} %pt_h.1, bf16[1,2048]{1,0:T(2,128)(2,1)} %dt_h.1, s32[1]{0:T(128)S(6)} %copy.21.pf_h, s32[1]{0:T(128)S(6)} %copy.22.df_h, bf16[544,256]{1,0:T(8,128)(2,1)} %bitcast.9, ...), custom_call_target="tpu_custom_call" | custom-call | tf_op jit(solution)/shard_map/pallas_call | solution.py:546
  46.9 0.6 %shard_map.193 = (bf16[4,2048]{1,0:T(4,128)(2,1)}, bf16[1,2048]{1,0:T(2,128)(2,1)}, bf16[4,544]{1,0:T(4,128)(2,1)}, bf16[1,544]{1,0:T(2,128)(2,1)}) custom-call(bf16[4,2048]{1,0:T(4,128)(2,1)S(1)} %get-tuple-element.8.refs_0_, bf16[1,2048]{1,0:T(2,128)(2,1)S(1)} %get-tuple-element.9.refs_1_, bf16[4,544]{1,0:T(4,128)(2,1)S(1)} %get-tuple-element.10.refs_2_, ...), custom_call_target="tpu_custom_call" | custom-call | tf_op jit(solution)/shard_map/pallas_call | solution.py:561
